TPU v7x, 32 devices: a whole 2x2x4 slice. The times are simulated.
32 devices in a mesh: grp: 2 (over x), ep: 16 (over z, y, core).
Axes of the slice: x: 2, y: 2, z: 4, core: 2. Of those that a mesh axis runs over, the one named last changes fastest.
Arguments:
- tokens: bfloat16 [1024, 2048], P(('grp', 'ep')), parts along dimension 0, may hold values from -6 to 6
- norm_gain: float32 [2048], replicated, may hold values from 0.1 to 1.9
- routing: int32 [1024, 8], P(('grp', 'ep')), parts along dimension 0, may hold values from 0 to 15, all different within a row; in each aligned block of 32 rows (0 to 31, 32 to 63, ...) at most 32 rows name the same one
- gates: float32 [1024, 8], P(('grp', 'ep')), parts along dimension 0, may hold values from 0.05 to 0.6
- w_gate: bfloat16 [16, 2048, 512], P('ep'), may hold values from -0.125 to 0.125
- w_up: bfloat16 [16, 2048, 512], P('ep'), may hold values from -0.125 to 0.125
- w_down: bfloat16 [16, 512, 2048], P('ep'), may hold values from -0.25 to 0.25
- shared_gate: bfloat16 [2048, 512], replicated, may hold values from -0.125 to 0.125
- shared_up: bfloat16 [2048, 512], replicated, may hold values from -0.125 to 0.125
- shared_down: bfloat16 [512, 2048], replicated, may hold values from -0.25 to 0.25
Outputs:
- mixed: bfloat16 [1024, 2048], P(('grp', 'ep')), parts along dimension 0
There are 2 independent parts, one for each index of `grp`. A program takes and returns all parts, laid end to end along the dimension named above; an argument that names none is the same for every part. Nothing has to cross between parts.
Inputs may be any that keep to these rules, and one draw needn't show every extreme that they name: `routing`: within the 32 rows of one device no expert is named by more than 32 rows, and in every draw some expert is named by exactly 32 rows of some device; each row names 8 different experts.
All inputs are finite; a program needn't handle non-finite values.
Results may differ from a plain program's by a relative error of at most 0.0067.
Values may be sent and summed in bfloat16 or wider, within the bound.
No kernel may reach another device: no remote copies, remote signals or barrier semaphores. Data moves between devices by JAX's collectives and lax.ppermute only.
A program may use at most 128 MiB of HBM per device.

v0:
```python
import jax
import jax.numpy as jnp
from jax import lax
from jax.sharding import PartitionSpec as P

epsilon = 1e-06


def rms_normed(tokens, norm_gain):
    floats = tokens.astype(jnp.float32)
    scale_inv = lax.rsqrt(jnp.mean(floats * floats, axis=-1, keepdims=True) + epsilon)
    return (floats * scale_inv * norm_gain).astype(jnp.bfloat16)


def expert_outputs(buffer, w_gate, w_up, w_down):
    gate_act = jnp.einsum("nesd,edf->nesf", buffer, w_gate, preferred_element_type=jnp.float32)
    up_act = jnp.einsum("nesd,edf->nesf", buffer, w_up, preferred_element_type=jnp.float32)
    hidden = (jax.nn.silu(gate_act) * up_act).astype(jnp.bfloat16)
    return jnp.einsum("nesf,efd->nesd", hidden, w_down, preferred_element_type=jnp.float32).astype(
        jnp.bfloat16
    )


def slot_targets(routing, expert_count, slot_count):
    leading = routing.shape[:-2]
    tok_count, top_count = routing.shape[-2:]
    flattened = routing.reshape(leading + (tok_count * top_count,))
    onehot = (flattened[..., None] == jnp.arange(expert_count, dtype=jnp.int32)).astype(jnp.int32)
    earlier = jnp.cumsum(onehot, axis=-2) - onehot
    within = jnp.sum(earlier * onehot, axis=-1)
    return (flattened * slot_count + within).reshape(routing.shape)


def slot_tables(targets, gates, row_count):
    slot_ids = jnp.arange(row_count, dtype=jnp.int32)
    matches = targets[..., None] == slot_ids
    selected = jnp.any(matches, axis=-2)
    weights = jnp.sum(
        jnp.where(matches, gates[..., None], jnp.zeros_like(gates[..., None])), axis=-2
    )
    return (selected, weights)


def body(
    tokens, norm_gain, routing, gates, w_gate, w_up, w_down, shared_gate, shared_up, shared_down
):
    normed = rms_normed(tokens, norm_gain)
    shared_hidden = (
        jax.nn.silu(jnp.dot(normed, shared_gate, preferred_element_type=jnp.float32))
        * jnp.dot(normed, shared_up, preferred_element_type=jnp.float32)
    ).astype(jnp.bfloat16)
    shared_out = jnp.dot(shared_hidden, shared_down, preferred_element_type=jnp.float32)
    tok_count, top_count = routing.shape
    local_count = w_gate.shape[0]
    ep_size = lax.axis_size("ep")
    expert_count = local_count * ep_size
    slot_count = max(4, (2 * tok_count * top_count + expert_count - 1) // expert_count)
    model_width = normed.shape[1]
    targets = slot_targets(routing, expert_count, slot_count)
    selected, weights = slot_tables(targets, gates, expert_count * slot_count)
    buffer = jnp.einsum(
        "tr,td->rd", selected.astype(jnp.bfloat16), normed, preferred_element_type=jnp.float32
    ).astype(jnp.bfloat16)
    buffer = buffer.reshape(ep_size, local_count, slot_count, model_width)
    returned = lax.all_to_all(
        expert_outputs(
            lax.all_to_all(buffer, "ep", split_axis=0, concat_axis=0, tiled=True),
            w_gate,
            w_up,
            w_down,
        ),
        "ep",
        split_axis=0,
        concat_axis=0,
        tiled=True,
    )
    returned = returned.reshape(expert_count * slot_count, model_width)
    chosen_rows = returned[targets.reshape(-1)].reshape(tok_count, top_count, model_width)
    routed = jnp.sum(gates[..., None] * chosen_rows.astype(jnp.float32), axis=1)
    return (shared_out + routed).astype(jnp.bfloat16)


def solution(mesh):
    placed = (
        P(("grp", "ep"), None),
        P(),
        P(("grp", "ep"), None),
        P(("grp", "ep"), None),
        P("ep", None, None),
        P("ep", None, None),
        P("ep", None, None),
        P(),
        P(),
        P(),
    )
    return jax.shard_map(
        body, mesh=mesh, in_specs=placed, out_specs=P(("grp", "ep"), None), check_vma=False
    )
```

profile of v0, /device:TPU:15, one launch (start us, length us, event | category | flops | bytes accessed | tf_op | source)
XLA Modules:
  0.0 129.9 jit_solution(7531492811068998764)
XLA Ops:
  0.0 0.0 copy-start
  0.0 0.9 copy.26
  0.9 0.1 eq.42
  1.0 0.1 eq.38
  1.1 0.6 reduce-window.6
  1.7 0.2 slice_reduce_fusion
  1.9 0.1 fusion.53
  2.0 0.1 reduce_sum.33
  2.1 0.2 fusion.41
  2.4 1.0 fusion.42
  3.4 1.7 %convolution_convert_fusion.1 = bf16[512,2048]{1,0:T(8,128)(2,1)S(1)} fusion(pred[32,512]{1,0:T(8,128)(4,1)S(1)} %fusion.41, bf16[32,2048]{1,0:T(8,128)(2,1)} %param.10, f32[2048]{0:T(1024)} %param.11, f32[32]{0:T(128)S(1)} %add_rsqrt_fusion), kind=kOutput, calls=%fused_computation.2 | convolution fusion | flops 68419584 | bytes 2252928 | tf_op jit(solution)/shard_map/tr,td->rd/dot_general | solution.py:61
  5.1 0.0 copy-start.5
  5.1 53.7 %all_to_all.10 = bf16[16,1,32,2048]{3,2,1,0:T(8,128)(2,1)S(1)} all-to-all(bf16[16,1,32,2048]{3,2,1,0:T(8,128)(2,1)S(1)} %bitcast.105), channel_id=1, replica_groups=mesh['grp'=2,'ep'=16] {'ep'}, dimensions={0} | all-to-all | bytes 4194304 | tf_op jit(solution)/shard_map/all_to_all | solution.py:67
  58.8 0.0 copy-start.2
  58.8 1.3 copy-done.2
  60.1 0.0 copy-done.5
  60.1 1.2 fusion.10
  61.4 0.0 copy-done
  61.4 6.1 %fusion = bf16[16,1,32,2048]{3,2,1,0:T(8,128)(2,1)} fusion(bf16[1,512,2048]{2,1,0:T(8,128)(2,1)S(1)} %copy-done, bf16[1,2048,512]{2,1,0:T(8,128)(2,1)} %param.15, bf16[16,1,32,2048]{3,2,1,0:T(8,128)(2,1)} %copy-done.2, f32[16,1,32,512]{3,2,0,1:T(8,128)S(1)} %fusion.10), kind=kOutput, calls=%fused_computation.3 | convolution fusion | flops 2150105088 | bytes 9437184 | tf_op jit(solution)/shard_map/nesf,efd->nesd/dot_general | solution.py:19
  67.5 0.0 copy-start.4
  67.5 0.0 copy-start.1
  67.5 0.0 copy-start.3
  67.5 5.2 %all-to-all-start.1 = ((bf16[16,1,32,2048]{3,2,1,0:T(8,128)(2,1)}), bf16[16,1,32,2048]{3,2,1,0:T(8,128)(2,1)}, u32[]{:S(2)}, u32[]{:S(2)}) async-start(bf16[16,1,32,2048]{3,2,1,0:T(8,128)(2,1)} %fusion), calls=%async_computation.1 | async-start | bytes 4194304 | tf_op jit(solution)/shard_map/all_to_all | solution.py:65
  72.6 0.1 mul.75
  72.7 0.0 copy-done.4
  72.7 0.7 copy.25
  73.4 0.0 copy-done.1
  73.4 0.0 copy-done.3
  73.4 2.7 %fusion.61 = f32[32,512]{1,0:T(8,128)} fusion(bf16[2048,512]{1,0:T(8,128)(2,1)} %param.17, bf16[32,2048]{1,0:T(8,128)(2,1)S(1)} %copy-done.1, f32[2048]{0:T(1024)S(1)} %copy-done.3, f32[32]{0:T(128)S(1)} %add_rsqrt_fusion), kind=kOutput, calls=%fused_computation.52 | convolution fusion | flops 67371008 | bytes 2302080 | tf_op jit(solution)/shard_map/dot_general | solution.py:49
  76.2 44.0 %all-to-all-done.1 = bf16[16,1,32,2048]{3,2,1,0:T(8,128)(2,1)} async-done(((bf16[16,1,32,2048]{3,2,1,0:T(8,128)(2,1)}), bf16[16,1,32,2048]{3,2,1,0:T(8,128)(2,1)}, u32[]{:S(2)}, u32[]{:S(2)}) %all-to-all-start.1) | async-done | bytes 2097184 | tf_op jit(solution)/shard_map/all_to_all | solution.py:65
  120.1 4.2 %gather_fusion = bf16[256,2048]{1,0:T(8,128)(2,1)S(1)} fusion(bf16[512,2048]{1,0:T(8,128)(2,1)} %bitcast.23, s32[1024]{0:T(1024)S(1)} %pad_clamp_fusion), kind=kCustom, calls=%fused_computation | custom fusion | bytes 2098176 | tf_op jit(solution)/shard_map/gather | solution.py:78
  124.4 1.7 %fusion.2 = f32[32,2048]{1,0:T(8,128)S(1)} fusion(bf16[256,2048]{1,0:T(8,128)(2,1)S(1)} %gather_fusion, f32[32,8]{1,0:T(8,128)} %copy.25), kind=kLoop, calls=%fused_computation.7 | loop fusion | flops 1507328 | bytes 1311744 | tf_op jit(solution)/shard_map/reduce_sum | solution.py:79
  126.1 3.9 %fusion.1 = bf16[32,2048]{1,0:T(8,128)(2,1)} fusion(f32[32,2048]{1,0:T(8,128)S(1)} %fusion.2, bf16[512,2048]{1,0:T(8,128)(2,1)} %param.19, bf16[2048,512]{1,0:T(8,128)(2,1)} %param.18, f32[32,512]{1,0:T(8,128)} %fusion.61, bf16[32,2048]{1,0:T(8,128)(2,1)S(1)} %copy-done.1, f32[2048]{0:T(1024)S(1)} %copy-done.3, f32[32]{0:T(128)S(1)} %add_rsqrt_fusion), kind=kOutput, calls=%fused_computation.5 | convolution fusion | flops 134709248 | bytes 4792448 | tf_op jit(solution)/shard_map/dot_general | solution.py:52
  (7 shorter events, 0.1 us)
Async XLA Ops:
  0.0 61.4 %copy-start = (bf16[1,512,2048]{2,1,0:T(8,128)(2,1)S(1)}, bf16[1,512,2048]{2,1,0:T(8,128)(2,1)}, u32[]{:S(2)}) copy-start(bf16[1,512,2048]{2,1,0:T(8,128)(2,1)} %param.16) | copy-start | bytes 6291460
  5.1 55.0 %copy-start.5 = (bf16[1,2048,512]{2,1,0:T(8,128)(2,1)S(1)}, bf16[1,2048,512]{2,1,0:T(8,128)(2,1)}, u32[]{:S(2)}) copy-start(bf16[1,2048,512]{2,1,0:T(8,128)(2,1)} %param.14) | copy-start | bytes 6291460
  58.8 1.3 copy-start.2
  67.5 5.3 %copy-start.4 = (f32[32,8]{0,1:T(8,128)S(1)}, f32[32,8]{0,1:T(8,128)}, u32[]{:S(2)}) copy-start(f32[32,8]{0,1:T(8,128)} %param.13) | copy-start | bytes 3076
  67.5 6.0 %copy-start.1 = (bf16[32,2048]{1,0:T(8,128)(2,1)S(1)}, bf16[32,2048]{1,0:T(8,128)(2,1)}, u32[]{:S(2)}) copy-start(bf16[32,2048]{1,0:T(8,128)(2,1)} %param.10) | copy-start | bytes 393220
  67.5 6.0 %copy-start.3 = (f32[2048]{0:T(1024)S(1)}, f32[2048]{0:T(1024)}, u32[]{:S(2)}) copy-start(f32[2048]{0:T(1024)} %param.11) | copy-start | bytes 24580
  67.5 52.7 %all-to-all-start.1 = ((bf16[16,1,32,2048]{3,2,1,0:T(8,128)(2,1)}), bf16[16,1,32,2048]{3,2,1,0:T(8,128)(2,1)}, u32[]{:S(2)}, u32[]{:S(2)}) async-start(bf16[16,1,32,2048]{3,2,1,0:T(8,128)(2,1)} %fusion), calls=%async_computation.1 | async-start | bytes 4194304 | tf_op jit(solution)/shard_map/all_to_all | solution.py:65
where the time goes:
time: 130 us
  blocking collectives  53.7 us (41%)
  waiting for transfers between devices  44 us (34%)
  matrix products  15.6 us (12%)
  local copies, waits for them, and re-layouts  7.66 us (6%)
  starting transfers between devices  5.17 us (4%)
  other arithmetic  3.72 us (3%)
    all_to_all x1, blocking collectives, body(): lax.all_to_all(buffer, 'ep', split_axis=0, concat_axis=0, tiled=True)  53.7 us
    all_to_all x1, waiting for transfers between devices, body(): lax.all_to_all(expert_outputs(lax.all_to_all(buffer, 'ep', split_axis=0,...  44 us
    dot_general x1, matrix products, expert_outputs(): jnp.einsum('nesf,efd->nesd', hidden, w_down, preferred_element_type=jnp.f...  6.06 us
    all_to_all x1, starting transfers between devices, body(): lax.all_to_all(expert_outputs(lax.all_to_all(buffer, 'ep', split_axis=0,...  5.17 us
    gather x1, local copies, waits for them, and re-layouts, body(): returned[targets.reshape(-1)].reshape(tok_count, top_count, model_width)  4.22 us
    dot_general x1, matrix products, body(): jnp.dot(shared_hidden, shared_down, preferred_element_type=jnp.float32)  3.87 us
    unnamed x14, local copies, waits for them, and re-layouts  2.91 us
    dot_general x1, matrix products, body(): jnp.dot(normed, shared_gate, preferred_element_type=jnp.float32)  2.74 us
  transfers between devices with their start and end apart: 1, of which 1 were waited for; matrix products, arithmetic and copies ran while one was open for 3% of the time, Pallas kernels for 0%

commit v1 on v0

v1 whole, which is shorter than its diff:
```python
import jax
import jax.numpy as jnp
from jax import lax
from jax.sharding import PartitionSpec as P

epsilon = 1e-06


def rms_normed(tokens, norm_gain):
    floats = tokens.astype(jnp.float32)
    scale_inv = lax.rsqrt(jnp.mean(floats * floats, axis=-1, keepdims=True) + epsilon)
    return (floats * scale_inv * norm_gain).astype(jnp.bfloat16)


def dense_gates(routing, gates, expert_count):
    ids = jnp.arange(expert_count, dtype=jnp.int32)
    matches = routing[..., None] == ids
    return jnp.sum(jnp.where(matches, gates[..., None], 0.0), axis=1)


def split3(values):
    def cut(v):
        return lax.reduce_precision(v, 8, 7)

    high = cut(values)
    middle = cut(values - high)
    low = values - high - middle
    return jnp.concatenate([high, middle, low], axis=1).astype(jnp.bfloat16)


def body(
    tokens, norm_gain, routing, gates, w_gate, w_up, w_down, shared_gate, shared_up, shared_down
):
    normed = rms_normed(tokens, norm_gain)
    width = normed.shape[1]
    local_count = w_gate.shape[0]
    ep_size = lax.axis_size("ep")
    expert_count = local_count * ep_size
    parts = split3(dense_gates(routing, gates, expert_count))
    parts = jnp.pad(parts, ((0, 0), (0, -parts.shape[1] % 128)))
    gathered = lax.all_gather(
        jnp.concatenate([normed, parts], axis=1), "ep", axis=0, tiled=True
    )
    shared_hidden = (
        jax.nn.silu(jnp.dot(normed, shared_gate, preferred_element_type=jnp.float32))
        * jnp.dot(normed, shared_up, preferred_element_type=jnp.float32)
    ).astype(jnp.bfloat16)
    shared_out = jnp.dot(shared_hidden, shared_down, preferred_element_type=jnp.float32)
    every = gathered[:, :width]
    split = gathered[:, width:].astype(jnp.float32)
    my_index = lax.axis_index("ep")
    total = None
    for i in range(local_count):
        expert = my_index * local_count + i
        columns = jnp.arange(split.shape[1], dtype=jnp.int32)
        mine = (columns % expert_count == expert) & (columns < 3 * expert_count)
        weight = jnp.sum(jnp.where(mine, split, 0.0), axis=1, keepdims=True)
        gate_act = jnp.dot(every, w_gate[i], preferred_element_type=jnp.float32)
        up_act = jnp.dot(every, w_up[i], preferred_element_type=jnp.float32)
        hidden = (jax.nn.silu(gate_act) * up_act).astype(jnp.bfloat16)
        out = jnp.dot(hidden, w_down[i], preferred_element_type=jnp.float32)
        out = weight * out
        total = out if total is None else total + out
    routed = lax.psum_scatter(
        total.astype(jnp.bfloat16), "ep", scatter_dimension=0, tiled=True
    )
    return (shared_out + routed.astype(jnp.float32)).astype(jnp.bfloat16)


def solution(mesh):
    placed = (
        P(("grp", "ep"), None),
        P(),
        P(("grp", "ep"), None),
        P(("grp", "ep"), None),
        P("ep", None, None),
        P("ep", None, None),
        P("ep", None, None),
        P(),
        P(),
        P(),
    )
    return jax.shard_map(
        body, mesh=mesh, in_specs=placed, out_specs=P(("grp", "ep"), None), check_vma=False
    )
```

time: 130 us -> 137 us (1.054)
  the two profiles are of different devices: /device:TPU:15 before, /device:TPU:0 now
where the time goes in v1:
time: 137 us
  waiting for transfers between devices  103 us (75%)
  matrix products  15.3 us (11%)
  between operations  13.4 us (10%)
  other arithmetic  4.66 us (3%)
    reduce_scatter x1, waiting for transfers between devices, body(): lax.psum_scatter(total.astype(jnp.bfloat16), 'ep', scatter_dimension=0, t...  58.3 us
    all_gather x1, waiting for transfers between devices, body(): lax.all_gather(jnp.concatenate([normed, parts], axis=1), 'ep', axis=0, ti...  44.7 us
    dot_general x1, matrix products, body(): out = jnp.dot(hidden, w_down[i], preferred_element_type=jnp.float32)  6.04 us
    dot_general x1, matrix products, body(): jnp.dot(shared_hidden, shared_down, preferred_element_type=jnp.float32)  3.78 us
    dot_general x1, matrix products, body(): gate_act = jnp.dot(every, w_gate[i], preferred_element_type=jnp.float32)  3.46 us
  transfers between devices with their start and end apart: 2, of which 2 were waited for; matrix products, arithmetic and copies ran while one was open for 1% of the time, Pallas kernels for 0%

profile of v1, /device:TPU:0, one launch (start us, length us, event | category | flops | bytes accessed | tf_op | source)
XLA Modules:
  0.0 136.7 jit_solution(15461209227420348828)
XLA Ops:
  6.5 0.0 copy-start
  6.5 0.0 all-gather.2.cloned.1.call-start
  6.5 0.9 select_reduce_fusion.1
  7.4 0.1 copy.14
  7.5 1.0 fusion.25
  8.6 1.0 fusion.27
  9.6 0.7 fusion.28
  10.3 0.0 all-gather.2.cloned.1.call-update
  10.3 0.0 reduce-scatter.2.cloned.1.call-start
  10.4 44.7 %all-gather.2.cloned.1.call-done = bf16[512,2176]{1,0:T(8,128)(2,1)} async-done(((bf16[32,2176]{1,0:T(8,128)(2,1)}), bf16[512,2176]{1,0:T(8,128)(2,1)}) %all-gather.2.cloned.1.call-update) | async-done | bytes 2228240 | tf_op jit(solution)/shard_map/all_gather | solution.py:41
  55.1 3.5 %fusion.4 = f32[512,512]{1,0:T(8,128)S(1)} fusion(bf16[1,2048,512]{2,1,0:T(8,128)(2,1)} %param.14, bf16[512,2176]{1,0:T(8,128)(2,1)} %all-gather.2.cloned.1.call-done), kind=kOutput, calls=%fused_computation.6 | convolution fusion | flops 1073741824 | bytes 5242880 | tf_op jit(solution)/shard_map/dot_general | solution.py:58
  58.6 1.0 select_reduce_fusion
  59.6 0.0 copy-done
  59.6 6.0 %multiply_convert_fusion = bf16[512,2048]{1,0:T(8,128)(2,1)} fusion(bf16[1,512,2048]{2,1,0:T(8,128)(2,1)S(1)} %copy-done, f32[512]{0:T(512)S(1)} %select_reduce_fusion, bf16[1,2048,512]{2,1,0:T(8,128)(2,1)} %param.15, bf16[512,2176]{1,0:T(8,128)(2,1)} %all-gather.2.cloned.1.call-done, f32[512,512]{1,0:T(8,128)S(1)} %fusion.4), kind=kOutput, calls=%fused_computation | convolution fusion | flops 2151153664 | bytes 9439232 | tf_op jit(solution)/shard_map/dot_general | solution.py:61
  65.6 0.0 reduce-scatter.2.cloned.1.call-update
  65.7 2.0 %fusion.38 = f32[32,512]{1,0:T(8,128)S(1)} fusion(bf16[32,2048]{1,0:T(8,128)(2,1)S(1)} %fusion.27, bf16[2048,512]{1,0:T(8,128)(2,1)} %param.17), kind=kOutput, calls=%fused_computation.43 | convolution fusion | flops 67108864 | bytes 2293760 | tf_op jit(solution)/shard_map/dot_general | solution.py:45
  67.7 58.3 %reduce-scatter.2.cloned.1.call-done = bf16[32,2048]{1,0:T(8,128)(2,1)} async-done(((bf16[512,2048]{1,0:T(8,128)(2,1)}), bf16[32,2048]{1,0:T(8,128)(2,1)}) %reduce-scatter.2.cloned.1.call-update) | async-done | bytes 131088 | tf_op jit(solution)/shard_map/reduce_scatter | solution.py:64
  126.0 3.8 %fusion = bf16[32,2048]{1,0:T(8,128)(2,1)} fusion(bf16[512,2048]{1,0:T(8,128)(2,1)} %param.19, bf16[32,2048]{1,0:T(8,128)(2,1)S(1)} %fusion.27, bf16[2048,512]{1,0:T(8,128)(2,1)} %param.18, bf16[32,2048]{1,0:T(8,128)(2,1)} %reduce-scatter.2.cloned.1.call-done, f32[32,512]{1,0:T(8,128)S(1)} %fusion.38), kind=kOutput, calls=%fused_computation.2 | convolution fusion | flops 134512640 | bytes 4653056 | tf_op jit(solution)/shard_map/dot_general | solution.py:48
  (4 shorter events, 0.0 us)
Async XLA Ops:
  6.5 53.1 %copy-start = (bf16[1,512,2048]{2,1,0:T(8,128)(2,1)S(1)}, bf16[1,512,2048]{2,1,0:T(8,128)(2,1)}, u32[]{:S(2)}) copy-start(bf16[1,512,2048]{2,1,0:T(8,128)(2,1)} %param.16) | copy-start | bytes 6291460
  6.5 48.6 %all-gather.2.cloned.1.call-start = ((), (), s32[]{:S(2)}) async-start(), calls=%async_computation.1 | async-start | bytes 2367488 | tf_op jit(solution)/shard_map/all_gather | solution.py:41
  10.3 115.7 %reduce-scatter.2.cloned.1.call-start = ((), (), s32[]{:S(2)}) async-start(), calls=%async_computation.2 | async-start | bytes 2228224 | tf_op jit(solution)/shard_map/reduce_scatter | solution.py:64
Sparse Core Ops, SparseCore 0:
  10.4 44.6 all-gather.1
  65.8 60.1 reduce-scatter.1
